TPU v7x, 32 devices: a whole 2x2x4 slice. The times are simulated.
32 devices in a mesh: ep: 8 (over z, x), tp: 4 (over y, core).
Axes of the slice: x: 2, y: 2, z: 4, core: 2. Of those that a mesh axis runs over, the one named last changes fastest.
Arguments:
- tokens: bfloat16 [1024, 2048], P('ep'), may hold values from -6 to 6
- routing: int32 [1024, 2], P('ep'), may hold values from 0 to 7, all different within a row; in each aligned block of 128 rows (0 to 127, 128 to 255, ...) at most 56 rows name the same one
- router_weight: bfloat16 [2048, 8], replicated, may hold values from -0.125 to 0.125
- gate_weight: bfloat16 [8, 2048, 2048], P('ep', None, 'tp'), may hold values from -0.125 to 0.125
- up_weight: bfloat16 [8, 2048, 2048], P('ep', None, 'tp'), may hold values from -0.125 to 0.125
- down_weight: bfloat16 [8, 2048, 2048], P('ep', 'tp'), may hold values from -0.125 to 0.125
- cotangent: bfloat16 [1024, 2048], P('ep'), may hold values from -0.796875 to 0.796875
Outputs:
- token_grad: bfloat16 [1024, 2048], P('ep')
- router_grad: float32 [2048, 8], P('tp')
- router_rows: float32 [2048], P('tp')
- gate_grad: bfloat16 [8, 2048, 2048], P('ep', None, 'tp')
- up_grad: bfloat16 [8, 2048, 2048], P('ep', None, 'tp')
- down_grad: bfloat16 [8, 2048, 2048], P('ep', 'tp')
- gate_rows: float32 [8, 2048], P('ep')
- up_rows: float32 [8, 2048], P('ep')
- down_rows: float32 [8, 2048], P('ep', 'tp')
Inputs may be any that keep to these rules, and one draw needn't show every extreme that they name: `routing`: A row's 2 experts differ. Within the rows of one index of ep (128 rows), no expert is named more than 56 times, a bound that some block reaches.
All inputs are finite; a program needn't handle non-finite values.
Results may differ from a plain program's by a relative error of at most 0.01.
Values may be sent and summed in bfloat16 or wider, within the bound.
A program may use at most 64 MiB of HBM per device.

v0:
```python
import jax
import jax.numpy as jnp
from jax import lax
from jax.sharding import PartitionSpec as P


def expert_backward(rows_in, cots_in, slot_scale, w_gate, w_up, w_down):
    pre_gate = jnp.dot(rows_in, w_gate, preferred_element_type=jnp.float32)
    pre_up = jnp.dot(rows_in, w_up, preferred_element_type=jnp.float32)
    sigmoid_gate = jax.nn.sigmoid(pre_gate)
    hidden = (pre_gate * sigmoid_gate * pre_up).astype(jnp.bfloat16)
    back_proj = lax.dot_general(
        cots_in, w_down, (((1,), (1,)), ((), ())), preferred_element_type=jnp.float32
    )
    gate_term = jnp.sum(hidden.astype(jnp.float32) * back_proj, axis=1)
    scaled = slot_scale * back_proj
    grad_up_pre = (scaled * pre_gate * sigmoid_gate).astype(jnp.bfloat16)
    grad_gate_pre = (
        scaled * pre_up * sigmoid_gate * (1.0 + pre_gate * (1.0 - sigmoid_gate))
    ).astype(jnp.bfloat16)
    weighted = (slot_scale * cots_in.astype(jnp.float32)).astype(jnp.bfloat16)
    contract_rows = (((0,), (0,)), ((), ()))
    grad_down = lax.dot_general(hidden, weighted, contract_rows, preferred_element_type=jnp.float32)
    grad_gate = lax.dot_general(
        rows_in, grad_gate_pre, contract_rows, preferred_element_type=jnp.float32
    )
    grad_up = lax.dot_general(
        rows_in, grad_up_pre, contract_rows, preferred_element_type=jnp.float32
    )
    contract_hidden = (((1,), (1,)), ((), ()))
    partial_value = lax.dot_general(
        grad_gate_pre, w_gate, contract_hidden, preferred_element_type=jnp.float32
    )
    partial_value = partial_value + lax.dot_general(
        grad_up_pre, w_up, contract_hidden, preferred_element_type=jnp.float32
    )
    return (partial_value, gate_term, grad_gate, grad_up, grad_down)


def per_device(tokens, routing, router_weight, gate_weight, up_weight, down_weight, cotangent):
    groups = lax.axis_size("ep")
    shares = lax.axis_size("tp")
    tok_count, model_width = tokens.shape
    top_count = routing.shape[1]
    local_experts = gate_weight.shape[0]
    experts = local_experts * groups
    capacity = 7 * tok_count * top_count // (4 * experts)
    slot_span = groups * capacity
    assigns = tok_count * top_count
    col_width = model_width // shares
    col_start = lax.axis_index("tp") * col_width
    logits = jnp.dot(tokens, router_weight, preferred_element_type=jnp.float32)
    affinity = jax.nn.sigmoid(logits)
    chosen = jnp.take_along_axis(affinity, routing, axis=1)
    total_aff = jnp.sum(chosen, axis=1, keepdims=True)
    weights = chosen / total_aff
    flat_ids = routing.reshape(-1)
    onehot_ids = (flat_ids[:, None] == jnp.arange(experts, dtype=jnp.int32)[None, :]).astype(
        jnp.int32
    )
    position = jnp.sum((jnp.cumsum(onehot_ids, axis=0) - 1) * onehot_ids, axis=1)
    slot_of = flat_ids % local_experts * slot_span + flat_ids // local_experts * capacity + position
    slot_table = jnp.full((local_experts * slot_span,), assigns, jnp.int32)
    slot_table = slot_table.at[slot_of].set(jnp.arange(assigns, dtype=jnp.int32))
    zero_row = jnp.zeros((1, model_width), jnp.bfloat16)
    tok_pad = jnp.concatenate([tokens, zero_row], axis=0)
    cot_pad = jnp.concatenate([cotangent, zero_row], axis=0)
    weight_pad = jnp.concatenate(
        [weights.astype(jnp.bfloat16).reshape(-1), jnp.zeros((1,), jnp.bfloat16)]
    )
    source_tok = slot_table // top_count
    rows_send = tok_pad[source_tok].reshape(local_experts, groups, capacity, model_width)
    cots_send = cot_pad[source_tok].reshape(local_experts, groups, capacity, model_width)
    scale_send = weight_pad[slot_table].reshape(local_experts, groups, capacity)
    rows_recv, cots_recv, scale_recv = (
        lax.all_to_all(rows_send, "ep", split_axis=1, concat_axis=1, tiled=True),
        lax.all_to_all(cots_send, "ep", split_axis=1, concat_axis=1, tiled=True),
        lax.all_to_all(scale_send, "ep", split_axis=1, concat_axis=1, tiled=True),
    )
    partials, gate_terms, gate_grads, up_grads, down_grads = ([], [], [], [], [])
    slot_scale = scale_recv[0].reshape(slot_span).astype(jnp.float32)[:, None]
    result = expert_backward(
        rows_recv[0].reshape(slot_span, model_width),
        cots_recv[0].reshape(slot_span, model_width),
        slot_scale,
        gate_weight[0],
        up_weight[0],
        down_weight[0],
    )
    partials.append(result[0])
    gate_terms.append(result[1])
    gate_grads.append(result[2])
    up_grads.append(result[3])
    down_grads.append(result[4])
    partial_value = jnp.stack(partials)
    gate_term = jnp.stack(gate_terms)
    grad_gate = jnp.stack(gate_grads)
    grad_up = jnp.stack(up_grads)
    grad_down = jnp.stack(down_grads)
    gate_rows, up_rows = lax.psum(
        (jnp.sum(grad_gate * grad_gate, axis=2), jnp.sum(grad_up * grad_up, axis=2)), "tp"
    )
    down_rows = jnp.sum(grad_down * grad_down, axis=2)
    summed = lax.psum_scatter(partial_value, "tp", scatter_dimension=2, tiled=True)
    gate_sum = lax.psum(gate_term, "tp")
    back_send = summed.astype(jnp.bfloat16).reshape(local_experts, groups, capacity, col_width)
    gate_send = gate_sum.astype(jnp.bfloat16).reshape(local_experts, groups, capacity)
    back_recv, gate_recv = (
        lax.all_to_all(back_send, "ep", split_axis=1, concat_axis=1, tiled=True),
        lax.all_to_all(gate_send, "ep", split_axis=1, concat_axis=1, tiled=True),
    )
    router_cols = lax.dynamic_slice_in_dim(router_weight, col_start, col_width, 0)
    back_flat = back_recv.reshape(local_experts * slot_span, -1)
    back_rows = jnp.sum(
        back_flat[slot_of].astype(jnp.float32).reshape(tok_count, top_count, -1), axis=1
    )
    d_weights = gate_recv.reshape(-1)[slot_of].astype(jnp.float32).reshape(tok_count, top_count)
    d_chosen = (d_weights - jnp.sum(d_weights * weights, axis=1, keepdims=True)) / total_aff
    d_logit = d_chosen * chosen * (1.0 - chosen)
    onehot = (routing[:, :, None] == jnp.arange(experts, dtype=jnp.int32)[None, None, :]).astype(
        jnp.float32
    )
    d_logits = jnp.sum(d_logit[:, :, None] * onehot, axis=1).astype(jnp.bfloat16)
    token_cols = lax.dynamic_slice_in_dim(tokens, col_start, col_width, 1)
    router_part = lax.dot_general(
        token_cols, d_logits, (((0,), (0,)), ((), ())), preferred_element_type=jnp.float32
    )
    router_grad = lax.psum(router_part, "ep")
    router_rows = jnp.sum(router_grad * router_grad, axis=1)
    router_back = lax.dot_general(
        d_logits, router_cols, (((1,), (1,)), ((), ())), preferred_element_type=jnp.float32
    )
    token_grad = (back_rows + router_back).astype(jnp.bfloat16)
    token_grad = lax.all_gather(token_grad, "tp", axis=1, tiled=True)
    return (
        token_grad,
        router_grad,
        router_rows,
        grad_gate.astype(jnp.bfloat16),
        grad_up.astype(jnp.bfloat16),
        grad_down.astype(jnp.bfloat16),
        gate_rows,
        up_rows,
        down_rows,
    )


def solution(mesh):
    return jax.shard_map(
        per_device,
        mesh=mesh,
        in_specs=(
            P("ep", None),
            P("ep", None),
            P(),
            P("ep", None, "tp"),
            P("ep", None, "tp"),
            P("ep", "tp", None),
            P("ep", None),
        ),
        out_specs=(
            P("ep", None),
            P("tp", None),
            P("tp"),
            P("ep", None, "tp"),
            P("ep", None, "tp"),
            P("ep", "tp", None),
            P("ep", None),
            P("ep", None),
            P("ep", "tp"),
        ),
        check_vma=False,
    )
```

profile of v0, /device:TPU:0, one launch (start us, length us, event | category | flops | bytes accessed | tf_op | source)
XLA Modules:
  0.0 255.0 jit_solution(7731860463774829727)
XLA Ops:
  16.6 3.2 %gather_fusion = bf16[448]{0:T(512)(128)(2,1)S(1)} fusion(bf16[257]{0:T(512)(128)(2,1)S(1)} %pad_maximum_fusion, s32[1024]{0:T(1024)S(1)} %get-tuple-element.83), kind=kCustom, calls=%fused_computation | custom fusion | bytes 3584 | tf_op jit(solution)/shard_map/gather | solution.py:74
  20.4 7.3 %all-to-all-start = ((bf16[1,8,56]{2,0,1:T(2,128)(2,1)}), bf16[1,8,56]{2,0,1:T(2,128)(2,1)S(1)}, u32[]{:S(2)}, u32[]{:S(2)}) async-start(bf16[1,8,56]{2,0,1:T(2,128)(2,1)} %reshape.229), calls=%async_computation | async-start | bytes 8192 | tf_op jit(solution)/shard_map/all_to_all | solution.py:78
  27.7 3.2 %gather_fusion.2 = bf16[448,2048]{1,0:T(8,128)(2,1)} fusion(bf16[129,2048]{1,0:T(8,128)(2,1)S(1)} %concatenate.11, s32[1024]{0:T(1024)S(1)} %get-tuple-element.82), kind=kCustom, calls=%fused_computation.2 | custom fusion | bytes 3671808 | tf_op jit(solution)/shard_map/gather | solution.py:72
  30.9 3.2 %all-to-all-done = bf16[1,8,56]{2,0,1:T(2,128)(2,1)S(1)} async-done(((bf16[1,8,56]{2,0,1:T(2,128)(2,1)}), bf16[1,8,56]{2,0,1:T(2,128)(2,1)S(1)}, u32[]{:S(2)}, u32[]{:S(2)}) %all-to-all-start) | async-done | bytes 928 | tf_op jit(solution)/shard_map/all_to_all | solution.py:78
  34.1 4.3 %all-to-all-start.2 = ((bf16[1,8,56,2048]{3,2,0,1:T(8,128)(2,1)}), bf16[1,8,56,2048]{3,2,0,1:T(8,128)(2,1)}, u32[]{:S(2)}, u32[]{:S(2)}) async-start(bf16[1,8,56,2048]{3,2,0,1:T(8,128)(2,1)} %bitcast.67), calls=%async_computation.2 | async-start | bytes 3670016 | tf_op jit(solution)/shard_map/all_to_all | solution.py:76
  39.5 3.2 %gather_fusion.1 = bf16[448,2048]{1,0:T(8,128)(2,1)} fusion(bf16[129,2048]{1,0:T(8,128)(2,1)S(1)} %concatenate.10, s32[1024]{0:T(1024)S(1)} %get-tuple-element.82), kind=kCustom, calls=%fused_computation.1 | custom fusion | bytes 3671808 | tf_op jit(solution)/shard_map/gather | solution.py:73
  42.7 37.2 %all-to-all-done.2 = bf16[1,8,56,2048]{3,2,0,1:T(8,128)(2,1)} async-done(((bf16[1,8,56,2048]{3,2,0,1:T(8,128)(2,1)}), bf16[1,8,56,2048]{3,2,0,1:T(8,128)(2,1)}, u32[]{:S(2)}, u32[]{:S(2)}) %all-to-all-start.2) | async-done | bytes 1835040 | tf_op jit(solution)/shard_map/all_to_all | solution.py:76
  79.9 4.3 %all-to-all-start.1 = ((bf16[1,8,56,2048]{3,2,0,1:T(8,128)(2,1)}), bf16[1,8,56,2048]{3,2,0,1:T(8,128)(2,1)}, u32[]{:S(2)}, u32[]{:S(2)}) async-start(bf16[1,8,56,2048]{3,2,0,1:T(8,128)(2,1)} %bitcast.66), calls=%async_computation.1 | async-start | bytes 3670016 | tf_op jit(solution)/shard_map/all_to_all | solution.py:77
  84.6 4.2 %fusion.5 = f32[448,512]{1,0:T(8,128)} fusion(bf16[448,2048]{1,0:T(8,128)(2,1)} %bitcast.11, bf16[1,2048,512]{2,1,0:T(8,128)(2,1)} %param.11), kind=kOutput, calls=%fused_computation.17 | convolution fusion | flops 939524096 | bytes 4849664 | tf_op jit(solution)/shard_map/dot_general | solution.py:9
  88.8 3.5 %fusion.2 = f32[448,512]{1,0:T(8,128)} fusion(bf16[448,2048]{1,0:T(8,128)(2,1)} %bitcast.11, bf16[1,2048,512]{2,1,0:T(8,128)(2,1)S(1)} %copy-done), kind=kOutput, calls=%fused_computation.14 | convolution fusion | flops 939524096 | bytes 4849664 | tf_op jit(solution)/shard_map/dot_general | solution.py:8
  92.3 34.1 %all-to-all-done.1 = bf16[1,8,56,2048]{3,2,0,1:T(8,128)(2,1)} async-done(((bf16[1,8,56,2048]{3,2,0,1:T(8,128)(2,1)}), bf16[1,8,56,2048]{3,2,0,1:T(8,128)(2,1)}, u32[]{:S(2)}, u32[]{:S(2)}) %all-to-all-start.1) | async-done | bytes 1835040 | tf_op jit(solution)/shard_map/all_to_all | solution.py:77
  126.4 5.5 %multiply_reduce_fusion.3 = (f32[448]{0:T(512)}, bf16[448,512]{1,0:T(8,128)(2,1)}, bf16[448,512]{1,0:T(8,128)(2,1)S(1)}, bf16[448,512]{1,0:T(8,128)(2,1)S(1)}) fusion(f32[448,512]{1,0:T(8,128)} %fusion.5, f32[448,512]{1,0:T(8,128)} %fusion.2, f32[448]{0:T(512)S(1)} %reshape.164, bf16[448,2048]{1,0:T(8,128)(2,1)} %bitcast.7, bf16[1,512,2048]{2,1,0:T(8,128)(2,1)} %param.12), kind=kOutput, calls=%fused_computation.32 | convolution fusion | flops 944111168 | bytes 7147008 | tf_op jit(solution)/shard_map/dot_general | solution.py:12
  133.5 3.0 %add_bitcast_fusion = f32[1,448,2048]{2,1,0:T(8,128)} fusion(f32[448,2048]{1,0:T(8,128)S(1)} %fusion, bf16[448,512]{1,0:T(8,128)(2,1)S(1)} %get-tuple-element.79, bf16[1,2048,512]{2,1,0:T(8,128)(2,1)S(1)} %copy-done.2), kind=kOutput, calls=%fused_computation.11 | convolution fusion | flops 940441600 | bytes 9895936 | tf_op jit(solution)/shard_map/dot_general | solution.py:34
  136.6 4.1 %convert_bitcast_fusion.2 = (bf16[1,2048,512]{1,2,0:T(8,128)(2,1)}, f32[2048]{0:T(1024)S(1)}) fusion(bf16[448,2048]{1,0:T(8,128)(2,1)} %bitcast.11, bf16[448,512]{1,0:T(8,128)(2,1)S(1)} %get-tuple-element.78), kind=kOutput, calls=%fused_computation.23 | convolution fusion | flops 942667776 | bytes 4399104 | tf_op jit(solution)/shard_map/dot_general | solution.py:24
  140.7 4.3 %convert_bitcast_fusion.1 = (bf16[1,2048,512]{1,2,0:T(8,128)(2,1)}, f32[2048]{0:T(1024)S(1)}) fusion(bf16[448,2048]{1,0:T(8,128)(2,1)} %bitcast.11, bf16[448,512]{1,0:T(8,128)(2,1)S(1)} %get-tuple-element.79), kind=kOutput, calls=%fused_computation.22 | convolution fusion | flops 942667776 | bytes 4399104 | tf_op jit(solution)/shard_map/dot_general | solution.py:27
  145.0 11.0 %all-reduce.2 = (bf16[1,448]{1,0:T(2,128)(2,1)S(1)}, f32[1,2048]{1,0:T(1,128)}, f32[1,2048]{1,0:T(1,128)}) all-reduce(f32[1,448]{1,0:T(1,128)S(1)} %bitcast.73, f32[1,2048]{1,0:T(1,128)S(1)} %bitcast.68, f32[1,2048]{1,0:T(1,128)S(1)} %bitcast.69), channel_id=1, replica_groups=mesh['ep'=8,'tp'=4] {'tp'}, use_global_device_ids=true, to_apply=%region_8.9 | all-reduce | flops 4544 | bytes 35456 | tf_op jit(solution)/shard_map/psum | solution.py:105
  156.7 4.5 %all-to-all-start.4 = ((bf16[1,8,56]{2,0,1:T(2,128)(2,1)}), bf16[1,8,56]{2,0,1:T(2,128)(2,1)S(1)}, u32[]{:S(2)}, u32[]{:S(2)}) async-start(bf16[1,8,56]{2,0,1:T(2,128)(2,1)} %reshape.230), calls=%async_computation.5 | async-start | bytes 8192 | tf_op jit(solution)/shard_map/all_to_all | solution.py:110
  161.3 15.6 %reduce-scatter.2.cloned.1.call-done = f32[1,448,512]{2,1,0:T(8,128)} async-done(((f32[1,448,2048]{2,1,0:T(8,128)}), f32[1,448,512]{2,1,0:T(8,128)}) %reduce-scatter.2.cloned.1.call-update) | async-done | bytes 917520 | tf_op jit(solution)/shard_map/reduce_scatter | solution.py:104
  178.9 5.5 %all-to-all-start.3 = ((bf16[1,8,56,512]{3,2,0,1:T(8,128)(2,1)}), bf16[1,8,56,512]{3,2,0,1:T(8,128)(2,1)S(1)}, u32[]{:S(2)}, u32[]{:S(2)}) async-start(bf16[1,8,56,512]{3,2,0,1:T(8,128)(2,1)} %bitcast.16), calls=%async_computation.4 | async-start | bytes 917504 | tf_op jit(solution)/shard_map/all_to_all | solution.py:109
  184.4 4.9 %multiply_reduce_fusion = (f32[512]{0:T(512)}, bf16[1,512,2048]{2,1,0:T(8,128)(2,1)}) fusion(bf16[448,512]{1,0:T(8,128)(2,1)} %get-tuple-element.67, bf16[448,2048]{1,0:T(8,128)(2,1)} %bitcast.7, f32[448]{0:T(512)S(1)} %copy-done.11), kind=kOutput, calls=%fused_computation.7 | convolution fusion | flops 945421824 | bytes 4394752 | tf_op jit(solution)/shard_map/dot_general | solution.py:23
  189.3 3.9 %copy.90 = bf16[1,2048,512]{2,1,0:T(8,128)(2,1)} copy(bf16[1,2048,512]{1,2,0:T(8,128)(2,1)} %get-tuple-element.76) | data formatting | bytes 4194304
  193.3 3.9 %copy.91 = bf16[1,2048,512]{2,1,0:T(8,128)(2,1)} copy(bf16[1,2048,512]{1,2,0:T(8,128)(2,1)} %get-tuple-element.74) | data formatting | bytes 4194304
  199.7 37.5 %psum.29 = f32[512,8]{0,1:T(8,128)S(1)} all-reduce(f32[512,8]{0,1:T(8,128)S(1)} %fusion.15), channel_id=1, replica_groups=mesh['ep'=8,'tp'=4] {'ep'}, use_global_device_ids=true, to_apply=%region_11.12 | all-reduce | flops 4096 | bytes 32768 | tf_op jit(solution)/shard_map/psum | solution.py:128
  240.9 6.5 %all_gather.3 = bf16[128,2048]{1,0:T(8,128)(2,1)S(1)} all-gather(bf16[128,512]{1,0:T(8,128)(2,1)S(1)} %fusion.11), channel_id=1, replica_groups=mesh['ep'=8,'tp'=4] {'tp'}, dimensions={1}, use_global_device_ids=true | all-gather | bytes 655360 | tf_op jit(solution)/shard_map/all_gather | solution.py:134
  (84 shorter events, 22.6 us)
Async XLA Ops:
  7.2 81.6 %copy-start = (bf16[1,2048,512]{2,1,0:T(8,128)(2,1)S(1)}, bf16[1,2048,512]{2,1,0:T(8,128)(2,1)}, u32[]{:S(2)}) copy-start(bf16[1,2048,512]{2,1,0:T(8,128)(2,1)} %param.10) | copy-start | bytes 6291460
  11.0 1.7 copy-start.7
  14.0 1.6 copy-start.4
  14.0 13.7 %copy-start.1 = (bf16[128,2048]{1,0:T(8,128)(2,1)S(1)}, bf16[128,2048]{1,0:T(8,128)(2,1)}, u32[]{:S(2)}) copy-start(bf16[128,2048]{1,0:T(8,128)(2,1)} %param.7) | copy-start | bytes 1572868
  15.6 15.3 %copy-start.5 = (f32[128]{0:T(128)}, f32[128]{0:T(128)S(1)}, u32[]{:S(2)}) copy-start(f32[128]{0:T(128)S(1)} %get-tuple-element.70) | copy-start | bytes 1540
  20.4 13.7 %all-to-all-start = ((bf16[1,8,56]{2,0,1:T(2,128)(2,1)}), bf16[1,8,56]{2,0,1:T(2,128)(2,1)S(1)}, u32[]{:S(2)}, u32[]{:S(2)}) async-start(bf16[1,8,56]{2,0,1:T(2,128)(2,1)} %reshape.229), calls=%async_computation | async-start | bytes 8192 | tf_op jit(solution)/shard_map/all_to_all | solution.py:78
  34.1 45.8 %all-to-all-start.2 = ((bf16[1,8,56,2048]{3,2,0,1:T(8,128)(2,1)}), bf16[1,8,56,2048]{3,2,0,1:T(8,128)(2,1)}, u32[]{:S(2)}, u32[]{:S(2)}) async-start(bf16[1,8,56,2048]{3,2,0,1:T(8,128)(2,1)} %bitcast.67), calls=%async_computation.2 | async-start | bytes 3670016 | tf_op jit(solution)/shard_map/all_to_all | solution.py:76
  79.9 46.5 %all-to-all-start.1 = ((bf16[1,8,56,2048]{3,2,0,1:T(8,128)(2,1)}), bf16[1,8,56,2048]{3,2,0,1:T(8,128)(2,1)}, u32[]{:S(2)}, u32[]{:S(2)}) async-start(bf16[1,8,56,2048]{3,2,0,1:T(8,128)(2,1)} %bitcast.66), calls=%async_computation.1 | async-start | bytes 3670016 | tf_op jit(solution)/shard_map/all_to_all | solution.py:77
  84.2 92.7 %reduce-scatter.2.cloned.1.call-start = ((), (), s32[]{:S(2)}) async-start(), calls=%async_computation.6 | async-start | bytes 4587520 | tf_op jit(solution)/shard_map/reduce_scatter | solution.py:104
  84.6 41.8 %copy-start.10 = (f32[448]{0:T(512)}, f32[448]{0:T(512)S(1)}, u32[]{:S(2)}) copy-start(f32[448]{0:T(512)S(1)} %reshape.164) | copy-start | bytes 5380
  131.9 1.6 copy-start.2
  140.7 4.3 %copy-start.12 = (f32[448]{0:T(512)S(1)}, f32[448]{0:T(512)}, u32[]{:S(2)}) copy-start(f32[448]{0:T(512)} %get-tuple-element.66) | copy-start | bytes 5380
  140.7 20.6 %copy-start.8 = (s32[256,1]{0,1:T(1,128)S(1)}, s32[256,1]{0,1:T(1,128)}, u32[]{:S(2)}) copy-start(s32[256,1]{0,1:T(1,128)} %copy-done.7) | copy-start | bytes 3076
  145.0 39.4 %copy-start.11 = (f32[448]{0:T(512)S(1)}, f32[448]{0:T(512)}, u32[]{:S(2)}) copy-start(f32[448]{0:T(512)} %copy-done.10) | copy-start | bytes 5380
  156.7 22.2 %all-to-all-start.4 = ((bf16[1,8,56]{2,0,1:T(2,128)(2,1)}), bf16[1,8,56]{2,0,1:T(2,128)(2,1)S(1)}, u32[]{:S(2)}, u32[]{:S(2)}) async-start(bf16[1,8,56]{2,0,1:T(2,128)(2,1)} %reshape.230), calls=%async_computation.5 | async-start | bytes 8192 | tf_op jit(solution)/shard_map/all_to_all | solution.py:110
  178.9 58.9 %all-to-all-start.3 = ((bf16[1,8,56,512]{3,2,0,1:T(8,128)(2,1)}), bf16[1,8,56,512]{3,2,0,1:T(8,128)(2,1)S(1)}, u32[]{:S(2)}, u32[]{:S(2)}) async-start(bf16[1,8,56,512]{3,2,0,1:T(8,128)(2,1)} %bitcast.16), calls=%async_computation.4 | async-start | bytes 917504 | tf_op jit(solution)/shard_map/all_to_all | solution.py:109
  193.3 6.2 %copy-start.9 = (f32[128,2]{0,1:T(2,128)S(1)}, f32[128,2]{0,1:T(2,128)}, u32[]{:S(2)}) copy-start(f32[128,2]{0,1:T(2,128)} %get-tuple-element.69) | copy-start | bytes 3076
  193.3 6.2 %copy-start.6 = (f32[128]{0:T(128)S(1)}, f32[128]{0:T(128)}, u32[]{:S(2)}) copy-start(f32[128]{0:T(128)} %copy-done.5) | copy-start | bytes 1540
  237.2 3.7 %copy-start.3 = (f32[512,8]{0,1:T(8,128)}, f32[512,8]{0,1:T(8,128)S(1)}, u32[]{:S(2)}) copy-start(f32[512,8]{0,1:T(8,128)S(1)} %psum.29) | copy-start | bytes 49156
Sparse Core Ops, SparseCore 0:
  136.7 40.1 reduce-scatter.1
where the time goes:
time: 256 us; the launch traced here: 255 us
  waiting for transfers between devices  90.1 us (35%)
  blocking collectives  55 us (21%)
  matrix products  33.1 us (13%)
  local copies, waits for them, and re-layouts  30 us (12%)
  starting transfers between devices  26.2 us (10%)
  between operations  14.3 us (6%)
  other arithmetic  6.23 us (2%)
    psum x1, blocking collectives, per_device(): router_grad = lax.psum(router_part, 'ep')  37.5 us
    all_to_all x1, waiting for transfers between devices, per_device(): lax.all_to_all(rows_send, 'ep', split_axis=1, concat_axis=1, tiled=True)  37.2 us
    all_to_all x1, waiting for transfers between devices, per_device(): lax.all_to_all(cots_send, 'ep', split_axis=1, concat_axis=1, tiled=True)  34.1 us
    reduce_scatter x1, waiting for transfers between devices, per_device(): lax.psum_scatter(partial_value, 'tp', scatter_dimension=2, tiled=True)  15.6 us
    psum x1, blocking collectives, per_device(): gate_sum = lax.psum(gate_term, 'tp')  11 us
    unnamed x30, local copies, waits for them, and re-layouts  9.92 us
    all_to_all x1, starting transfers between devices, per_device(): lax.all_to_all(scale_send, 'ep', split_axis=1, concat_axis=1, tiled=True)  7.28 us
    all_gather x1, blocking collectives, per_device(): token_grad = lax.all_gather(token_grad, 'tp', axis=1, tiled=True)  6.5 us
  transfers between devices with their start and end apart: 6, of which 4 were waited for; matrix products, arithmetic and copies ran while one was open for 17% of the time, Pallas kernels for 0%

commit v1 on v0

--- a/solution.py
+++ b/solution.py
@@ -125,7 +125,7 @@
     router_part = lax.dot_general(
         token_cols, d_logits, (((0,), (0,)), ((), ())), preferred_element_type=jnp.float32
     )
-    router_grad = lax.psum(router_part, "ep")
+    router_grad = jnp.sum(lax.all_gather(router_part, "ep"), axis=0)
     router_rows = jnp.sum(router_grad * router_grad, axis=1)
     router_back = lax.dot_general(
         d_logits, router_cols, (((1,), (1,)), ((), ())), preferred_element_type=jnp.float32

time: 256 us -> 240 us (0.938)
  waiting for transfers between devices: 90.1 us -> 74.5 us
    psum x1 -> x0, blocking collectives: 37.5 us -> none  [per_device(): router_grad = lax.psum(router_part, 'ep')]
    all_gather x0 -> x1, blocking collectives: none -> 34.9 us  [per_device(): router_grad = jnp.sum(lax.all_gather(router_part, 'ep'), axis=0)]
    reduce_scatter x1, waiting for transfers between devices: 15.6 us -> 0.01 us  [per_device(): lax.psum_scatter(partial_value, 'tp', scatter_dimension=2, tiled=True)]
    unnamed x30 -> x26, local copies, waits for them, and re-layouts: 9.92 us -> 9.94 us
  transfers between devices with their start and end apart: 6 -> 6, of which waited for: 4 -> 3; matrix products, arithmetic and copies ran while one was open for 17% -> 17% of each run, Pallas kernels for 0% -> 0%
where the time goes in v1:
time: 240 us; the launch traced here: 239 us
  waiting for transfers between devices  74.5 us (31%)
  blocking collectives  52.7 us (22%)
  matrix products  33.8 us (14%)
  local copies, waits for them, and re-layouts  30 us (12%)
  starting transfers between devices  26.8 us (11%)
  between operations  14.3 us (6%)
  other arithmetic  6.94 us (3%)
    all_to_all x1, waiting for transfers between devices, per_device(): lax.all_to_all(rows_send, 'ep', split_axis=1, concat_axis=1, tiled=True)  37.2 us
    all_gather x1, blocking collectives, per_device(): router_grad = jnp.sum(lax.all_gather(router_part, 'ep'), axis=0)  34.9 us
    all_to_all x1, waiting for transfers between devices, per_device(): lax.all_to_all(cots_send, 'ep', split_axis=1, concat_axis=1, tiled=True)  34.1 us
    psum x1, blocking collectives, per_device(): gate_sum = lax.psum(gate_term, 'tp')  10.9 us
    unnamed x26, local copies, waits for them, and re-layouts  9.94 us
    all_to_all x1, starting transfers between devices, per_device(): lax.all_to_all(scale_send, 'ep', split_axis=1, concat_axis=1, tiled=True)  7.28 us
    all_gather x1, blocking collectives, per_device(): token_grad = lax.all_gather(token_grad, 'tp', axis=1, tiled=True)  7.01 us
    all_to_all x1, starting transfers between devices, per_device(): lax.all_to_all(back_send, 'ep', split_axis=1, concat_axis=1, tiled=True)  5.98 us
  transfers between devices with their start and end apart: 6, of which 3 were waited for; matrix products, arithmetic and copies ran while one was open for 17% of the time, Pallas kernels for 0%

profile of v1, /device:TPU:0, one launch (start us, length us, event | category | flops | bytes accessed | tf_op | source)
XLA Modules:
  0.0 239.1 jit_solution(15628139852367422740)
XLA Ops:
  16.6 3.2 %gather_fusion = bf16[448]{0:T(512)(128)(2,1)S(1)} fusion(bf16[257]{0:T(512)(128)(2,1)S(1)} %pad_maximum_fusion, s32[1024]{0:T(1024)S(1)} %get-tuple-element.83), kind=kCustom, calls=%fused_computation | custom fusion | bytes 3584 | tf_op jit(solution)/shard_map/gather | solution.py:74
  20.4 7.3 %all-to-all-start = ((bf16[1,8,56]{2,0,1:T(2,128)(2,1)}), bf16[1,8,56]{2,0,1:T(2,128)(2,1)S(1)}, u32[]{:S(2)}, u32[]{:S(2)}) async-start(bf16[1,8,56]{2,0,1:T(2,128)(2,1)} %reshape.230), calls=%async_computation | async-start | bytes 8192 | tf_op jit(solution)/shard_map/all_to_all | solution.py:78
  27.8 3.2 %gather_fusion.2 = bf16[448,2048]{1,0:T(8,128)(2,1)} fusion(bf16[129,2048]{1,0:T(8,128)(2,1)S(1)} %concatenate.11, s32[1024]{0:T(1024)S(1)} %get-tuple-element.82), kind=kCustom, calls=%fused_computation.2 | custom fusion | bytes 3671808 | tf_op jit(solution)/shard_map/gather | solution.py:72
  30.9 3.2 %all-to-all-done = bf16[1,8,56]{2,0,1:T(2,128)(2,1)S(1)} async-done(((bf16[1,8,56]{2,0,1:T(2,128)(2,1)}), bf16[1,8,56]{2,0,1:T(2,128)(2,1)S(1)}, u32[]{:S(2)}, u32[]{:S(2)}) %all-to-all-start) | async-done | bytes 928 | tf_op jit(solution)/shard_map/all_to_all | solution.py:78
  34.1 4.3 %all-to-all-start.2 = ((bf16[1,8,56,2048]{3,2,0,1:T(8,128)(2,1)}), bf16[1,8,56,2048]{3,2,0,1:T(8,128)(2,1)}, u32[]{:S(2)}, u32[]{:S(2)}) async-start(bf16[1,8,56,2048]{3,2,0,1:T(8,128)(2,1)} %bitcast.68), calls=%async_computation.2 | async-start | bytes 3670016 | tf_op jit(solution)/shard_map/all_to_all | solution.py:76
  39.5 3.2 %gather_fusion.1 = bf16[448,2048]{1,0:T(8,128)(2,1)} fusion(bf16[129,2048]{1,0:T(8,128)(2,1)S(1)} %concatenate.10, s32[1024]{0:T(1024)S(1)} %get-tuple-element.82), kind=kCustom, calls=%fused_computation.1 | custom fusion | bytes 3671808 | tf_op jit(solution)/shard_map/gather | solution.py:73
  42.7 37.2 %all-to-all-done.2 = bf16[1,8,56,2048]{3,2,0,1:T(8,128)(2,1)} async-done(((bf16[1,8,56,2048]{3,2,0,1:T(8,128)(2,1)}), bf16[1,8,56,2048]{3,2,0,1:T(8,128)(2,1)}, u32[]{:S(2)}, u32[]{:S(2)}) %all-to-all-start.2) | async-done | bytes 1835040 | tf_op jit(solution)/shard_map/all_to_all | solution.py:76
  79.9 4.3 %all-to-all-start.1 = ((bf16[1,8,56,2048]{3,2,0,1:T(8,128)(2,1)}), bf16[1,8,56,2048]{3,2,0,1:T(8,128)(2,1)}, u32[]{:S(2)}, u32[]{:S(2)}) async-start(bf16[1,8,56,2048]{3,2,0,1:T(8,128)(2,1)} %bitcast.67), calls=%async_computation.1 | async-start | bytes 3670016 | tf_op jit(solution)/shard_map/all_to_all | solution.py:77
  84.6 4.2 %fusion.5 = f32[448,512]{1,0:T(8,128)} fusion(bf16[448,2048]{1,0:T(8,128)(2,1)} %bitcast.11, bf16[1,2048,512]{2,1,0:T(8,128)(2,1)} %param.11), kind=kOutput, calls=%fused_computation.17 | convolution fusion | flops 939524096 | bytes 4849664 | tf_op jit(solution)/shard_map/dot_general | solution.py:9
  88.8 3.5 %fusion.2 = f32[448,512]{1,0:T(8,128)} fusion(bf16[448,2048]{1,0:T(8,128)(2,1)} %bitcast.11, bf16[1,2048,512]{2,1,0:T(8,128)(2,1)S(1)} %copy-done), kind=kOutput, calls=%fused_computation.14 | convolution fusion | flops 939524096 | bytes 4849664 | tf_op jit(solution)/shard_map/dot_general | solution.py:8
  92.3 34.1 %all-to-all-done.1 = bf16[1,8,56,2048]{3,2,0,1:T(8,128)(2,1)} async-done(((bf16[1,8,56,2048]{3,2,0,1:T(8,128)(2,1)}), bf16[1,8,56,2048]{3,2,0,1:T(8,128)(2,1)}, u32[]{:S(2)}, u32[]{:S(2)}) %all-to-all-start.1) | async-done | bytes 1835040 | tf_op jit(solution)/shard_map/all_to_all | solution.py:77
  126.4 5.5 %multiply_reduce_fusion.3 = (f32[448]{0:T(512)}, bf16[448,512]{1,0:T(8,128)(2,1)}, bf16[448,512]{1,0:T(8,128)(2,1)S(1)}, bf16[448,512]{1,0:T(8,128)(2,1)S(1)}) fusion(f32[448,512]{1,0:T(8,128)} %fusion.5, f32[448,512]{1,0:T(8,128)} %fusion.2, f32[448]{0:T(512)S(1)} %reshape.164, bf16[448,2048]{1,0:T(8,128)(2,1)} %bitcast.7, bf16[1,512,2048]{2,1,0:T(8,128)(2,1)} %param.12), kind=kOutput, calls=%fused_computation.32 | convolution fusion | flops 944111168 | bytes 7147008 | tf_op jit(solution)/shard_map/dot_general | solution.py:12
  133.5 3.0 %add_bitcast_fusion = f32[1,448,2048]{2,1,0:T(8,128)} fusion(f32[448,2048]{1,0:T(8,128)S(1)} %fusion, bf16[448,512]{1,0:T(8,128)(2,1)S(1)} %get-tuple-element.79, bf16[1,2048,512]{2,1,0:T(8,128)(2,1)S(1)} %copy-done.2), kind=kOutput, calls=%fused_computation.11 | convolution fusion | flops 940441600 | bytes 9895936 | tf_op jit(solution)/shard_map/dot_general | solution.py:34
  137.2 4.7 %convert_bitcast_fusion.2 = (bf16[1,2048,512]{1,2,0:T(8,128)(2,1)}, f32[2048]{0:T(1024)}) fusion(bf16[448,2048]{1,0:T(8,128)(2,1)} %bitcast.11, bf16[448,512]{1,0:T(8,128)(2,1)S(1)} %get-tuple-element.78), kind=kOutput, calls=%fused_computation.23 | convolution fusion | flops 942667776 | bytes 4399104 | tf_op jit(solution)/shard_map/dot_general | solution.py:24
  142.0 4.4 %convert_bitcast_fusion.1 = (bf16[1,2048,512]{1,2,0:T(8,128)(2,1)}, f32[2048]{0:T(1024)S(1)}) fusion(bf16[448,2048]{1,0:T(8,128)(2,1)} %bitcast.11, bf16[448,512]{1,0:T(8,128)(2,1)S(1)} %get-tuple-element.79), kind=kOutput, calls=%fused_computation.22 | convolution fusion | flops 942667776 | bytes 4399104 | tf_op jit(solution)/shard_map/dot_general | solution.py:27
  146.3 10.9 %all-reduce.2 = (bf16[1,448]{1,0:T(2,128)(2,1)S(1)}, f32[1,2048]{1,0:T(1,128)}, f32[1,2048]{1,0:T(1,128)}) all-reduce(f32[1,448]{1,0:T(1,128)S(1)} %bitcast.75, f32[1,2048]{1,0:T(1,128)S(1)} %bitcast.70, f32[1,2048]{1,0:T(1,128)S(1)} %bitcast.71), channel_id=1, replica_groups=mesh['ep'=8,'tp'=4] {'tp'}, use_global_device_ids=true, to_apply=%region_8.9 | all-reduce | flops 4544 | bytes 35456 | tf_op jit(solution)/shard_map/psum | solution.py:105
  157.9 4.7 %all-to-all-start.4 = ((bf16[1,8,56]{2,0,1:T(2,128)(2,1)}), bf16[1,8,56]{2,0,1:T(2,128)(2,1)S(1)}, u32[]{:S(2)}, u32[]{:S(2)}) async-start(bf16[1,8,56]{2,0,1:T(2,128)(2,1)} %reshape.231), calls=%async_computation.5 | async-start | bytes 8192 | tf_op jit(solution)/shard_map/all_to_all | solution.py:110
  162.6 4.9 %multiply_reduce_fusion = (f32[512]{0:T(512)}, bf16[1,512,2048]{2,1,0:T(8,128)(2,1)}) fusion(bf16[448,512]{1,0:T(8,128)(2,1)} %get-tuple-element.67, bf16[448,2048]{1,0:T(8,128)(2,1)} %bitcast.7, f32[448]{0:T(512)S(1)} %copy-done.9), kind=kOutput, calls=%fused_computation.7 | convolution fusion | flops 945421824 | bytes 4394752 | tf_op jit(solution)/shard_map/dot_general | solution.py:23
  167.6 3.9 %copy.90 = bf16[1,2048,512]{2,1,0:T(8,128)(2,1)} copy(bf16[1,2048,512]{1,2,0:T(8,128)(2,1)} %get-tuple-element.76) | data formatting | bytes 4194304
  171.5 3.9 %copy.91 = bf16[1,2048,512]{2,1,0:T(8,128)(2,1)} copy(bf16[1,2048,512]{1,2,0:T(8,128)(2,1)} %get-tuple-element.74) | data formatting | bytes 4194304
  177.7 2.0 convert_element_type.94
  179.7 6.0 %all-to-all-start.3 = ((bf16[1,8,56,512]{3,2,0,1:T(8,128)(2,1)}), bf16[1,8,56,512]{3,2,0,1:T(8,128)(2,1)S(1)}, u32[]{:S(2)}, u32[]{:S(2)}) async-start(bf16[1,8,56,512]{3,2,0,1:T(8,128)(2,1)} %bitcast.16), calls=%async_computation.4 | async-start | bytes 917504 | tf_op jit(solution)/shard_map/all_to_all | solution.py:109
  185.9 34.9 %all-gather = f32[4096,8]{0,1:T(8,128)S(1)} all-gather(f32[512,8]{0,1:T(8,128)S(1)} %fusion.15), channel_id=2, replica_groups=mesh['ep'=8,'tp'=4] {'ep'}, dimensions={0}, use_global_device_ids=true | all-gather | bytes 147456 | tf_op jit(solution)/shard_map/all_gather | solution.py:128
  224.4 7.0 %all_gather.9 = bf16[128,2048]{1,0:T(8,128)(2,1)S(1)} all-gather(bf16[128,512]{1,0:T(8,128)(2,1)S(1)} %fusion.11), channel_id=1, replica_groups=mesh['ep'=8,'tp'=4] {'tp'}, dimensions={1}, use_global_device_ids=true | all-gather | bytes 655360 | tf_op jit(solution)/shard_map/all_gather | solution.py:134
  (81 shorter events, 21.3 us)
Async XLA Ops:
  7.2 81.6 %copy-start = (bf16[1,2048,512]{2,1,0:T(8,128)(2,1)S(1)}, bf16[1,2048,512]{2,1,0:T(8,128)(2,1)}, u32[]{:S(2)}) copy-start(bf16[1,2048,512]{2,1,0:T(8,128)(2,1)} %param.10) | copy-start | bytes 6291460
  11.0 1.4 copy-start.6
  14.0 1.6 copy-start.4
  14.0 13.7 %copy-start.1 = (bf16[128,2048]{1,0:T(8,128)(2,1)S(1)}, bf16[128,2048]{1,0:T(8,128)(2,1)}, u32[]{:S(2)}) copy-start(bf16[128,2048]{1,0:T(8,128)(2,1)} %param.7) | copy-start | bytes 1572868
  20.4 13.7 %all-to-all-start = ((bf16[1,8,56]{2,0,1:T(2,128)(2,1)}), bf16[1,8,56]{2,0,1:T(2,128)(2,1)S(1)}, u32[]{:S(2)}, u32[]{:S(2)}) async-start(bf16[1,8,56]{2,0,1:T(2,128)(2,1)} %reshape.230), calls=%async_computation | async-start | bytes 8192 | tf_op jit(solution)/shard_map/all_to_all | solution.py:78
  34.1 45.8 %all-to-all-start.2 = ((bf16[1,8,56,2048]{3,2,0,1:T(8,128)(2,1)}), bf16[1,8,56,2048]{3,2,0,1:T(8,128)(2,1)}, u32[]{:S(2)}, u32[]{:S(2)}) async-start(bf16[1,8,56,2048]{3,2,0,1:T(8,128)(2,1)} %bitcast.68), calls=%async_computation.2 | async-start | bytes 3670016 | tf_op jit(solution)/shard_map/all_to_all | solution.py:76
  79.9 46.5 %all-to-all-start.1 = ((bf16[1,8,56,2048]{3,2,0,1:T(8,128)(2,1)}), bf16[1,8,56,2048]{3,2,0,1:T(8,128)(2,1)}, u32[]{:S(2)}, u32[]{:S(2)}) async-start(bf16[1,8,56,2048]{3,2,0,1:T(8,128)(2,1)} %bitcast.67), calls=%async_computation.1 | async-start | bytes 3670016 | tf_op jit(solution)/shard_map/all_to_all | solution.py:77
  84.2 93.5 %reduce-scatter.2.cloned.1.call-start = ((), (), s32[]{:S(2)}) async-start(), calls=%async_computation.6 | async-start | bytes 4587520 | tf_op jit(solution)/shard_map/reduce_scatter | solution.py:104
  84.6 41.8 %copy-start.8 = (f32[448]{0:T(512)}, f32[448]{0:T(512)S(1)}, u32[]{:S(2)}) copy-start(f32[448]{0:T(512)S(1)} %reshape.164) | copy-start | bytes 5380
  131.9 1.6 copy-start.2
  142.0 4.4 %copy-start.5 = (f32[2048]{0:T(1024)S(1)}, f32[2048]{0:T(1024)}, u32[]{:S(2)}) copy-start(f32[2048]{0:T(1024)} %get-tuple-element.77) | copy-start | bytes 24580
  142.0 4.4 %copy-start.10 = (f32[448]{0:T(512)S(1)}, f32[448]{0:T(512)}, u32[]{:S(2)}) copy-start(f32[448]{0:T(512)} %get-tuple-element.66) | copy-start | bytes 5380
  142.0 20.7 %copy-start.9 = (f32[448]{0:T(512)S(1)}, f32[448]{0:T(512)}, u32[]{:S(2)}) copy-start(f32[448]{0:T(512)} %copy-done.8) | copy-start | bytes 5380
  157.9 17.5 %all-to-all-start.4 = ((bf16[1,8,56]{2,0,1:T(2,128)(2,1)}), bf16[1,8,56]{2,0,1:T(2,128)(2,1)S(1)}, u32[]{:S(2)}, u32[]{:S(2)}) async-start(bf16[1,8,56]{2,0,1:T(2,128)(2,1)} %reshape.231), calls=%async_computation.5 | async-start | bytes 8192 | tf_op jit(solution)/shard_map/all_to_all | solution.py:110
  175.4 10.3 %copy-start.7 = (f32[128,2]{0,1:T(2,128)S(1)}, f32[128,2]{0,1:T(2,128)}, u32[]{:S(2)}) copy-start(f32[128,2]{0,1:T(2,128)} %get-tuple-element.69) | copy-start | bytes 3076
  179.7 41.7 %all-to-all-start.3 = ((bf16[1,8,56,512]{3,2,0,1:T(8,128)(2,1)}), bf16[1,8,56,512]{3,2,0,1:T(8,128)(2,1)S(1)}, u32[]{:S(2)}, u32[]{:S(2)}) async-start(bf16[1,8,56,512]{3,2,0,1:T(8,128)(2,1)} %bitcast.16), calls=%async_computation.4 | async-start | bytes 917504 | tf_op jit(solution)/shard_map/all_to_all | solution.py:109
  220.8 3.7 %copy-start.3 = (f32[512,8]{0,1:T(8,128)}, f32[512,8]{0,1:T(8,128)S(1)}, u32[]{:S(2)}) copy-start(f32[512,8]{0,1:T(8,128)S(1)} %reduce_sum.114) | copy-start | bytes 49156
Sparse Core Ops, SparseCore 0:
  136.7 40.2 reduce-scatter.1
